TPU v7x, 256 devices: a whole 4x4x8 slice. The times are simulated.
256 devices in a mesh: ep: 64 (over z, y, core), tp: 4 (over x).
Axes of the slice: x: 4, y: 4, z: 8, core: 2. Of those that a mesh axis runs over, the one named last changes fastest.
Arguments:
- resid: bfloat16 [2048, 2048], P('ep'), may hold values from -6 to 6
- mix_gain: bfloat16 [2048], replicated, may hold values from 0.099609375 to 1.8984375
- proj_x: bfloat16 [2048, 512], P(None, 'tp'), may hold values from -0.125 to 0.125
- proj_z: bfloat16 [2048, 512], P(None, 'tp'), may hold values from -0.125 to 0.125
- proj_b: bfloat16 [2048, 512], P(None, 'tp'), may hold values from -0.125 to 0.125
- proj_c: bfloat16 [2048, 512], P(None, 'tp'), may hold values from -0.125 to 0.125
- proj_step: bfloat16 [2048, 8], replicated, may hold values from -0.125 to 0.125
- step_bias: float32 [8], P('tp'), may hold values from -5 to -1
- decay_rate: float32 [8], P('tp'), may hold values from 1 to 16
- conv_taps: bfloat16 [3, 4, 512], P(None, None, 'tp'), may hold values from -3 to 3
- conv_state: bfloat16 [2048, 3, 3, 512], P('ep', None, None, 'tp'), may hold values from -6 to 6
- scan_state: float32 [2048, 8, 64, 128], P('ep', 'tp'), may hold values from -2.5 to 2.5
- inner_gain: bfloat16 [512], P('tp'), may hold values from 0.099609375 to 1.8984375
- proj_out: bfloat16 [512, 2048], P('tp'), may hold values from -0.25 to 0.25
- post_gain: bfloat16 [2048], replicated, may hold values from 0.099609375 to 1.8984375
- ffn_gain: bfloat16 [2048], replicated, may hold values from 0.099609375 to 1.8984375
- group_router: bfloat16 [2048, 2], replicated, may hold values from -0.125 to 0.125
- expert_router: bfloat16 [2048, 64], replicated, may hold values from -0.125 to 0.125
- route_experts: int32 [2048, 4], P('ep'), may hold values from 0 to 63, as said below
- expert_gate: bfloat16 [64, 2048, 1024], P('ep', None, 'tp'), may hold values from -0.125 to 0.125
- expert_up: bfloat16 [64, 2048, 1024], P('ep', None, 'tp'), may hold values from -0.125 to 0.125
- expert_down: bfloat16 [64, 1024, 2048], P('ep', 'tp')
- dense_switch: bfloat16 [2048], replicated, may hold values from -0.125 to 0.125
- dense_gate: bfloat16 [2048, 2048], P('ep', 'tp'), may hold values from -0.125 to 0.125
- dense_up: bfloat16 [2048, 2048], P('ep', 'tp'), may hold values from -0.125 to 0.125
- dense_down: bfloat16 [2048, 2048], P('ep', 'tp')
- out_gain: bfloat16 [2048], P('tp'), may hold values from 0.099609375 to 1.8984375
Outputs:
- layer_out: bfloat16 [2048, 2048], P('ep', 'tp')
- new_state: float32 [2048, 8, 64, 128], P('ep', 'tp')
- new_conv: bfloat16 [2048, 3, 3, 512], P('ep', None, None, 'tp')
Inputs may be any that keep to these rules, and one draw needn't show every extreme that they name: `route_experts`: each row names 4 different experts, all from one group of 32 consecutive expert numbers. Within each aligned block of 32 rows (the rows of one index of ep) no expert is named more than 4 times, and one expert, the same in every block, is named exactly 4 times in every block.
All inputs are finite; a program needn't handle non-finite values.
Results may differ from a plain program's by a relative error of at most 0.019.
Values may be sent and summed in bfloat16 or wider, within the bound.
No kernel may reach another device: no remote copies, remote signals or barrier semaphores. Data moves between devices by JAX's collectives and lax.ppermute only.
A program may use at most 64 MiB of HBM per device.

v0:
```python
import jax
import jax.numpy as jnp
from jax import lax
from jax.sharding import Mesh
from jax.sharding import PartitionSpec as P

EP = ("ep_0", "ep_1", "ep_2")
norm_eps = 1e-06


def sent_to_all(array, axis):
    count = lax.axis_size(axis)
    return lax.all_to_all(
        jnp.broadcast_to(array[None], (count, *array.shape)), axis, 0, 0, tiled=True
    )


def taken_together(array, axis):
    return sent_to_all(array, axis).astype(jnp.float32).sum(axis=0)


def cut_along(array, dim, count):
    shape = array.shape
    pieces = array.reshape(*shape[:dim], count, shape[dim] // count, *shape[dim + 1 :])
    return jnp.moveaxis(pieces, dim, 0)


def sum_at_owner(array, axis, dim):
    count = lax.axis_size(axis)
    pieces = lax.all_to_all(cut_along(array, dim, count), axis, 0, 0, tiled=True)
    return jnp.sum(pieces.astype(jnp.float32), axis=0)


def laid_out(pieces, dim):
    shape = list(pieces.shape[1:])
    shape[dim] *= pieces.shape[0]
    return jnp.moveaxis(pieces, 0, dim).reshape(shape)


def exchange_in_order(pieces, axes, sequence):
    inside = pieces.shape[1:]
    result = pieces.reshape(*(lax.axis_size(a) for a in axes), *inside)
    for k in sequence:
        result = lax.all_to_all(result, axes[k], k, k, tiled=True)
    return result.reshape(-1, *inside)


def two_step_exchange(array, groups, sequence, split_dim, concat_dim):
    count = lax.axis_size(groups[0]) * lax.axis_size(groups[1])
    pieces = cut_along(array, split_dim, count)
    return laid_out(exchange_in_order(pieces, groups, sequence), concat_dim)


def gather_directly(array, axis, dim):
    return laid_out(sent_to_all(array, axis), dim)


def sent_together(arrays, axis, dim, along):
    widths = [a.shape[along] for a in arrays]
    both = jnp.concatenate(arrays, axis=along)
    result = lax.all_gather(both, axis, axis=dim, tiled=True)
    return tuple(jnp.split(result, [sum(widths[:k]) for k in range(1, len(widths))], axis=along))


def all_blocks(array, axes, sequence):
    pieces = array[None]
    for k in sequence:
        pieces = lax.all_gather(pieces, axes[k], axis=0, tiled=True)
    block = [lax.axis_size(axes[k]) for k in reversed(sequence)]
    pieces = pieces.reshape(*block, *array.shape)
    turned = sorted(range(len(sequence)), key=lambda place: sequence[len(sequence) - 1 - place])
    return pieces.transpose(*turned, *range(len(sequence), pieces.ndim)).reshape(-1, *array.shape)


def gathered_by_axis(array, axes, sequence, dim):
    return laid_out(all_blocks(array, axes, sequence), dim)


def taken_together_2(array, axis):
    return sent_to_all(array, axis).sum(axis=0)


def scaled_rows(values, gain):
    values = values.astype(jnp.float32)
    mean_square = jnp.mean(values * values, axis=-1, keepdims=True)
    return values * lax.rsqrt(mean_square + norm_eps) * gain.astype(jnp.float32)


def softmax_plain(logits):
    weights = jnp.exp(logits)
    return weights / jnp.sum(weights, axis=-1, keepdims=True)


def on_device(
    resid,
    mix_gain,
    proj_x,
    proj_z,
    proj_b,
    proj_c,
    proj_step,
    step_bias,
    decay_rate,
    conv_taps,
    conv_state,
    scan_state,
    inner_gain,
    proj_out,
    post_gain,
    ffn_gain,
    group_router,
    expert_router,
    route_experts,
    expert_gate,
    expert_up,
    expert_down,
    dense_switch,
    dense_gate,
    dense_up,
    dense_down,
    out_gain,
):
    tp_index = lax.axis_index("tp")
    seqs = resid.shape[0]
    width = resid.shape[1]
    quarter = width // lax.axis_size("tp")
    heads_here = scan_state.shape[1]
    head_dim = scan_state.shape[2]
    state_dim = scan_state.shape[3]
    channels = conv_state.shape[3]
    repeat = heads_here // (channels // state_dim)
    normed = scaled_rows(resid, mix_gain).astype(jnp.bfloat16)
    fresh = jnp.stack(
        [
            jnp.dot(normed, proj_x, preferred_element_type=jnp.float32),
            jnp.dot(normed, proj_b, preferred_element_type=jnp.float32),
            jnp.dot(normed, proj_c, preferred_element_type=jnp.float32),
        ],
        axis=1,
    ).astype(jnp.bfloat16)
    gate_z = jnp.dot(normed, proj_z, preferred_element_type=jnp.float32)
    step_all = jnp.dot(normed, proj_step, preferred_element_type=jnp.float32)
    step_raw = lax.dynamic_slice_in_dim(step_all, tp_index * heads_here, heads_here, 1)
    history = jnp.concatenate([conv_state, fresh[:, :, None, :]], axis=2)
    activated = jax.nn.silu(
        jnp.sum(history.astype(jnp.float32) * conv_taps.astype(jnp.float32)[None], axis=2)
    )
    xs_heads = activated[:, 0].reshape(seqs, heads_here, head_dim)
    b_heads = jnp.repeat(activated[:, 1].reshape(seqs, -1, state_dim), repeat, axis=1)
    c_heads = jnp.repeat(activated[:, 2].reshape(seqs, -1, state_dim), repeat, axis=1)
    step = jax.nn.softplus(step_raw + step_bias)
    keep = jnp.exp(-decay_rate * step)
    driven = step[:, :, None] * xs_heads
    new_state = keep[:, :, None, None] * scan_state + driven[:, :, :, None] * b_heads[:, :, None, :]
    read = jnp.sum(new_state * c_heads[:, :, None, :], axis=3).reshape(seqs, channels)
    gated = (read * jax.nn.silu(gate_z) * inner_gain.astype(jnp.float32)).astype(jnp.bfloat16)
    mixed = taken_together(
        jnp.dot(gated, proj_out, preferred_element_type=jnp.float32).astype(jnp.bfloat16), "tp"
    ).astype(jnp.float32)
    stream = (resid.astype(jnp.float32) + scaled_rows(mixed, post_gain)).astype(jnp.bfloat16)
    feed = scaled_rows(stream, ffn_gain).astype(jnp.bfloat16)
    feed_quarter = lax.dynamic_slice_in_dim(feed, tp_index * quarter, quarter, 1)
    expert_count = expert_router.shape[1]
    group_size = expert_count // group_router.shape[1]
    pick_count = route_experts.shape[1]
    group_prob = softmax_plain(jnp.dot(feed, group_router, preferred_element_type=jnp.float32))
    expert_logits = jnp.dot(feed, expert_router, preferred_element_type=jnp.float32)
    matches = route_experts[:, :, None] == jnp.arange(expert_count, dtype=jnp.int32)[None, None, :]
    pick_logits = jnp.sum(jnp.where(matches, expert_logits[:, None, :], 0.0), axis=2)
    chosen_group = route_experts[:, 0] // group_size
    group_ids = jnp.arange(group_router.shape[1], dtype=jnp.int32)
    group_weight = jnp.sum(
        jnp.where(chosen_group[:, None] == group_ids[None, :], group_prob, 0.0), axis=1
    )
    pick_weight = softmax_plain(pick_logits) * group_weight[:, None]
    capacity = 2 * seqs * pick_count // expert_count
    flat_picks = route_experts.reshape(-1)
    one_hot = (flat_picks[:, None] == jnp.arange(expert_count, dtype=jnp.int32)[None, :]).astype(
        jnp.int32
    )
    slot = jnp.sum((jnp.cumsum(one_hot, axis=0) - one_hot) * one_hot, axis=1)
    target = flat_picks * capacity + slot
    repeated = jnp.repeat(feed_quarter, pick_count, axis=0)
    outgoing = jnp.zeros((expert_count * capacity, quarter), jnp.bfloat16).at[target].set(repeated)
    outgoing = outgoing.reshape(expert_count, capacity, quarter)
    arrived = gather_directly(
        lax.all_to_all(outgoing, EP, split_axis=0, concat_axis=0, tiled=True), "tp", 2
    )
    sources = arrived.shape[0]
    items = arrived.shape[1]
    rows = arrived.reshape(sources * items, width)
    gate_value = jnp.dot(rows, expert_gate[0], preferred_element_type=jnp.float32)
    up_value = jnp.dot(rows, expert_up[0], preferred_element_type=jnp.float32)
    hidden = (jax.nn.silu(gate_value) * up_value).astype(jnp.bfloat16)
    result = jnp.dot(hidden, expert_down[0], preferred_element_type=jnp.float32).reshape(
        sources, items, width
    )
    summed = sum_at_owner(result.astype(jnp.bfloat16), "tp", 2)
    returned = two_step_exchange(
        summed.astype(jnp.bfloat16), (("ep_0", "ep_1"), "ep_2"), (1, 0), 0, 0
    )
    fetched = returned.reshape(expert_count * capacity, quarter)[target].reshape(
        seqs, pick_count, quarter
    )
    routed = jnp.sum(fetched.astype(jnp.float32) * pick_weight[:, :, None], axis=1)
    pieces = sent_together((dense_gate, dense_up), EP, 0, 1)
    gate_piece = jnp.einsum(
        "sd,cd->sc", feed_quarter, pieces[0], preferred_element_type=jnp.float32
    )
    up_piece = jnp.einsum("sd,cd->sc", feed_quarter, pieces[1], preferred_element_type=jnp.float32)
    gate_sum = gate_piece
    up_sum = up_piece
    gate_sum, up_sum = (
        taken_together(gate_sum.astype(jnp.bfloat16), "tp").astype(jnp.float32),
        taken_together(up_sum.astype(jnp.bfloat16), "tp").astype(jnp.float32),
    )
    dense_hidden = (jax.nn.silu(gate_sum) * up_sum).astype(jnp.bfloat16)
    dense_out = jnp.dot(
        dense_hidden,
        gathered_by_axis(dense_down, EP, (1, 0, 2), 0),
        preferred_element_type=jnp.float32,
    )
    switch = jax.nn.sigmoid(jnp.dot(feed, dense_switch, preferred_element_type=jnp.float32))
    combined = routed + switch[:, None] * dense_out
    total_square = taken_together_2(jnp.sum(combined * combined, axis=1), "tp")
    scale = lax.rsqrt(total_square / width + norm_eps)
    stream_part = lax.dynamic_slice_in_dim(stream, tp_index * quarter, quarter, 1).astype(
        jnp.float32
    )
    layer_out = (stream_part + combined * scale[:, None] * out_gain.astype(jnp.float32)).astype(
        jnp.bfloat16
    )
    new_conv = history[:, :, 1:, :]
    return (layer_out, new_state, new_conv)


def solution(mesh):
    torus = Mesh(mesh.devices.reshape(8, 4, 2, mesh.shape["tp"]), ("ep_0", "ep_1", "ep_2", "tp"))
    in_specs = (
        P(EP, None),
        P(),
        P(None, "tp"),
        P(None, "tp"),
        P(None, "tp"),
        P(None, "tp"),
        P(),
        P("tp"),
        P("tp"),
        P(None, None, "tp"),
        P(EP, None, None, "tp"),
        P(EP, "tp", None, None),
        P("tp"),
        P("tp", None),
        P(),
        P(),
        P(),
        P(),
        P(EP, None),
        P(EP, None, "tp"),
        P(EP, None, "tp"),
        P(EP, "tp", None),
        P(),
        P(EP, "tp"),
        P(EP, "tp"),
        P(EP, "tp"),
        P("tp"),
    )
    out_specs = (P(EP, "tp"), P(EP, "tp", None, None), P(EP, None, None, "tp"))
    return jax.shard_map(
        on_device, mesh=torus, in_specs=in_specs, out_specs=out_specs, check_vma=False
    )
```

profile of v0, /device:TPU:32, one launch (start us, length us, event | category | flops | bytes accessed | tf_op | source)
XLA Modules:
  0.0 196.0 jit_solution(9819140083257767766)
XLA Ops:
  7.3 14.3 %all-gather = bf16[128,512]{1,0:T(8,128)(2,1)} all-gather(bf16[32,512]{1,0:T(8,128)(2,1)} %param.52), channel_id=2, replica_groups=mesh['ep_0'=8,'ep_1'=4,'ep_2'=2,'tp'=4] {'ep_1'}, dimensions={0}, use_global_device_ids=true | all-gather | bytes 163840 | tf_op jit(solution)/shard_map/all_gather | solution.py:68
  21.7 1.4 pad_maximum_fusion
  23.1 0.7 convert_element_type.93
  23.8 0.7 convert_element_type.96
  24.5 1.0 fusion.18
  25.6 1.4 fusion.4
  27.0 1.4 fusion.5
  28.3 1.4 fusion.6
  29.7 0.7 multiply_reduce_fusion.3
  30.6 0.2 fusion.39
  31.1 0.1 broadcast_multiply_fusion
  31.2 2.1 %multiply_reduce_fusion = (f32[32,2,64]{2,1,0:T(2,128)S(1)}, f32[32,2,64,128]{3,2,1,0:T(8,128)}) fusion(f32[32,128]{1,0:T(8,128)S(1)} %get-tuple-element.12, f32[32,128]{1,0:T(8,128)S(1)} %get-tuple-element.13, f32[32,2,64]{2,1,0:T(2,128)S(1)} %broadcast_multiply_fusion, f32[32,2,64,128]{3,2,1,0:T(8,128)S(1)} %copy-done.2, f32[32,2]{1,0:T(8,128)S(1)} %copy.73), kind=kLoop, calls=%fused_computation.8 | loop fusion | flops 2617344 | bytes 4260096 | tf_op jit(solution)/shard_map/reduce_sum | solution.py:155
  33.5 1.7 convolution_convert_fusion.3
  35.2 0.9 broadcast_in_dim.25
  36.0 4.3 %all-to-all-start = ((bf16[4,32,2048]{2,1,0:T(8,128)(2,1)}), bf16[4,32,2048]{2,1,0:T(8,128)(2,1)S(1)}, u32[]{:S(2)}, u32[]{:S(2)}) async-start(bf16[4,32,2048]{2,1,0:T(8,128)(2,1)} %broadcast_in_dim.25), calls=%async_computation | async-start | bytes 1048576 | tf_op jit(solution)/shard_map/all_to_all | solution.py:13
  40.7 0.2 reduce_window_sum.11
  41.0 0.2 select_reduce_fusion.1
  41.2 7.2 %all-to-all-done = bf16[4,32,2048]{2,1,0:T(8,128)(2,1)S(1)} async-done(((bf16[4,32,2048]{2,1,0:T(8,128)(2,1)}), bf16[4,32,2048]{2,1,0:T(8,128)(2,1)S(1)}, u32[]{:S(2)}, u32[]{:S(2)}) %all-to-all-start) | async-done | bytes 524320 | tf_op jit(solution)/shard_map/all_to_all | solution.py:13
  48.5 0.1 multiply_reduce_fusion.2
  48.6 0.2 fusion.15
  48.9 0.1 fusion.17
  49.1 1.1 scatter_custom_fusion
  50.3 22.3 %all_to_all.46 = bf16[64,4,512]{2,1,0:T(4,128)(2,1)S(1)} all-to-all(bf16[64,4,512]{2,1,0:T(4,128)(2,1)S(1)} %reshape.201), channel_id=1, replica_groups=mesh['ep_0'=8,'ep_1'=4,'ep_2'=2,'tp'=4] {'ep_0','ep_1','ep_2'}, dimensions={0} | all-to-all | bytes 524288 | tf_op jit(solution)/shard_map/all_to_all | solution.py:187
  72.6 0.3 broadcast_in_dim.28
  72.9 18.5 %all_to_all.47 = bf16[4,64,4,512]{3,2,1,0:T(4,128)(2,1)S(1)} all-to-all(bf16[4,64,4,512]{3,2,1,0:T(4,128)(2,1)S(1)} %broadcast_in_dim.28), channel_id=1, replica_groups=mesh['ep_0'=8,'ep_1'=4,'ep_2'=2,'tp'=4] {'tp'}, dimensions={0} | all-to-all | bytes 2097152 | tf_op jit(solution)/shard_map/all_to_all | solution.py:13
  91.4 1.4 copy.77
  92.7 0.3 copy.88
  93.0 0.4 fusion.13
  93.5 0.5 copy-done.14
  94.0 0.4 fusion.2
  94.5 0.4 convolution_convert_fusion
  94.9 1.1 copy.92
  96.0 3.6 %all-to-all-start.3 = ((bf16[4,64,4,512]{3,1,2,0:T(8,128)(2,1)}), bf16[4,64,4,512]{3,1,2,0:T(8,128)(2,1)S(1)}, u32[]{:S(2)}, u32[]{:S(2)}) async-start(bf16[4,64,4,512]{3,1,2,0:T(8,128)(2,1)} %bitcast.77), calls=%async_computation.3 | async-start | bytes 2097152 | tf_op jit(solution)/shard_map/all_to_all | solution.py:30
  99.7 0.7 all-gather.9.cloned.1.call-update
  100.5 0.2 fusion.47
  100.6 0.2 fusion.48
  100.8 13.7 %all-to-all-done.3 = bf16[4,64,4,512]{3,1,2,0:T(8,128)(2,1)S(1)} async-done(((bf16[4,64,4,512]{3,1,2,0:T(8,128)(2,1)}), bf16[4,64,4,512]{3,1,2,0:T(8,128)(2,1)S(1)}, u32[]{:S(2)}, u32[]{:S(2)}) %all-to-all-start.3) | async-done | bytes 1048608 | tf_op jit(solution)/shard_map/all_to_all | solution.py:30
  114.6 0.2 reduce_sum.166
  114.8 0.1 reshape_reshape.10
  114.9 0.2 copy.81
  115.1 3.9 %all_to_all.48 = bf16[32,2,1,4,512]{4,3,0,2,1:T(4,128)(2,1)S(1)} all-to-all(bf16[32,2,1,4,512]{4,3,0,2,1:T(4,128)(2,1)S(1)} %copy.81), channel_id=1, replica_groups=mesh['ep_0'=8,'ep_1'=4,'ep_2'=2,'tp'=4] {'ep_2'}, dimensions={1} | all-to-all | bytes 524288 | tf_op jit(solution)/shard_map/all_to_all | solution.py:44
  119.0 0.8 copy.82
  119.8 4.6 %all-to-all-start.5 = ((bf16[32,2,1,4,512]{4,3,1,2,0:T(4,128)(2,1)}), bf16[32,2,1,4,512]{4,3,1,2,0:T(4,128)(2,1)S(1)}, u32[]{:S(2)}, u32[]{:S(2)}) async-start(bf16[32,2,1,4,512]{4,3,1,2,0:T(4,128)(2,1)} %copy.82), calls=%async_computation.5 | async-start | bytes 524288 | tf_op jit(solution)/shard_map/all_to_all | solution.py:44
  124.4 0.2 select_reduce_fusion
  124.6 19.8 %all-gather.5.cloned.1.call-done = bf16[2048,1024]{1,0:T(8,128)(2,1)} async-done(((bf16[32,1024]{1,0:T(8,128)(2,1)}), bf16[2048,1024]{1,0:T(8,128)(2,1)}) %all-gather.5.cloned.1.call-update) | async-done | bytes 4194320 | tf_op jit(solution)/shard_map/all_gather | solution.py:61
  144.4 2.3 %convolution_convert_fusion.1 = bf16[32,2048]{1,0:T(8,128)(2,1)S(1)} fusion(bf16[32,512]{1,0:T(8,128)(2,1)S(1)} %constant_dynamic-slice_fusion, bf16[2048,1024]{1,0:T(8,128)(2,1)} %all-gather.5.cloned.1.call-done), kind=kOutput, calls=%fused_computation.3 | convolution fusion | flops 67174400 | bytes 2260992 | tf_op jit(solution)/shard_map/sd,cd->sc/dot_general | solution.py:210
  146.7 0.8 broadcast_in_dim.37
  147.6 4.2 %all-to-all-start.7 = ((bf16[4,32,2048]{2,1,0:T(8,128)(2,1)}), bf16[4,32,2048]{2,1,0:T(8,128)(2,1)S(1)}, u32[]{:S(2)}, u32[]{:S(2)}) async-start(bf16[4,32,2048]{2,1,0:T(8,128)(2,1)} %broadcast_in_dim.37), calls=%async_computation.7 | async-start | bytes 1048576 | tf_op jit(solution)/shard_map/all_to_all | solution.py:13
  151.9 2.3 %convolution_convert_fusion.2 = bf16[32,2048]{1,0:T(8,128)(2,1)S(1)} fusion(bf16[32,512]{1,0:T(8,128)(2,1)S(1)} %constant_dynamic-slice_fusion, bf16[2048,1024]{1,0:T(8,128)(2,1)} %all-gather.5.cloned.1.call-done), kind=kOutput, calls=%fused_computation.4 | convolution fusion | flops 67174400 | bytes 2260992 | tf_op jit(solution)/shard_map/sd,cd->sc/dot_general | solution.py:207
  154.2 7.5 %all-to-all-done.7 = bf16[4,32,2048]{2,1,0:T(8,128)(2,1)S(1)} async-done(((bf16[4,32,2048]{2,1,0:T(8,128)(2,1)}), bf16[4,32,2048]{2,1,0:T(8,128)(2,1)S(1)}, u32[]{:S(2)}, u32[]{:S(2)}) %all-to-all-start.7) | async-done | bytes 524320 | tf_op jit(solution)/shard_map/all_to_all | solution.py:13
  161.6 0.9 broadcast_in_dim.35
  162.6 4.1 %all-to-all-start.6 = ((bf16[4,32,2048]{2,1,0:T(8,128)(2,1)}), bf16[4,32,2048]{2,1,0:T(8,128)(2,1)}, u32[]{:S(2)}, u32[]{:S(2)}) async-start(bf16[4,32,2048]{2,1,0:T(8,128)(2,1)} %broadcast_in_dim.35), calls=%async_computation.6 | async-start | bytes 1048576 | tf_op jit(solution)/shard_map/all_to_all | solution.py:13
  166.7 0.1 fusion.10
  167.0 0.8 gather_fusion
  167.9 0.9 multiply_reduce_fusion.1
  168.8 1.8 copy.84
  170.7 5.1 %all-to-all-done.6 = bf16[4,32,2048]{2,1,0:T(8,128)(2,1)} async-done(((bf16[4,32,2048]{2,1,0:T(8,128)(2,1)}), bf16[4,32,2048]{2,1,0:T(8,128)(2,1)}, u32[]{:S(2)}, u32[]{:S(2)}) %all-to-all-start.6) | async-done | bytes 524320 | tf_op jit(solution)/shard_map/all_to_all | solution.py:13
  175.8 1.1 convert_reduce_fusion.1
  176.9 2.0 %multiply_reduce_fusion.4 = (f32[32]{0:T(128)S(1)}, f32[32,512]{1,0:T(8,128)}) fusion(f32[32,512]{1,0:T(8,128)} %multiply_reduce_fusion.1, bf16[2048,512]{1,0:T(8,128)(2,1)S(1)} %bitcast.78, f32[32,2048]{1,0:T(8,128)S(1)} %convert_reduce_fusion, f32[32,2048]{1,0:T(8,128)S(1)} %convert_reduce_fusion.1, f32[32]{0:T(128)S(1)} %fusion.10), kind=kOutput, calls=%fused_computation.57 | convolution fusion | flops 67567584 | bytes 2752768 | tf_op jit(solution)/shard_map/dot_general | solution.py:218
  178.9 0.6 broadcast_in_dim.39
  179.5 3.2 %all-to-all-start.8 = ((f32[4,1,32]{2,1,0:T(1,128)}), f32[4,1,32]{2,1,0:T(1,128)S(1)}, u32[]{:S(2)}, u32[]{:S(2)}) async-start(f32[4,1,32]{2,1,0:T(1,128)} %broadcast_in_dim.39), calls=%async_computation.8 | async-start | bytes 4096 | tf_op jit(solution)/shard_map/all_to_all | solution.py:13
  182.7 1.5 slice.31
  184.3 3.6 %all-to-all-done.8 = f32[4,1,32]{2,1,0:T(1,128)S(1)} async-done(((f32[4,1,32]{2,1,0:T(1,128)}), f32[4,1,32]{2,1,0:T(1,128)S(1)}, u32[]{:S(2)}, u32[]{:S(2)}) %all-to-all-start.8) | async-done | bytes 544 | tf_op jit(solution)/shard_map/all_to_all | solution.py:13
  187.9 1.5 add_convert_fusion
  (85 shorter events, 2.0 us)
Async XLA Ops:
  7.2 87.3 %copy-start = (bf16[1,256,2048]{2,1,0:T(8,128)(2,1)S(1)}, bf16[1,256,2048]{2,1,0:T(8,128)(2,1)}, u32[]{:S(2)}) copy-start(bf16[1,256,2048]{2,1,0:T(8,128)(2,1)} %param.48) | copy-start | bytes 3145732
  7.2 23.4 %copy-start.1 = (bf16[32,2048]{1,0:T(8,128)(2,1)S(1)}, bf16[32,2048]{1,0:T(8,128)(2,1)}, u32[]{:S(2)}) copy-start(bf16[32,2048]{1,0:T(8,128)(2,1)} %param.27) | copy-start | bytes 393220
  7.2 22.5 %copy-start.7 = (bf16[32,3,3,128]{3,0,2,1:T(8,128)(2,1)S(1)}, bf16[32,3,3,128]{3,0,2,1:T(8,128)(2,1)}, u32[]{:S(2)}) copy-start(bf16[32,3,3,128]{3,0,2,1:T(8,128)(2,1)} %param.37) | copy-start | bytes 221188
  7.2 23.3 %copy-start.17 = (f32[2]{0:T(128)S(1)}, f32[2]{0:T(128)}, u32[]{:S(2)}) copy-start(f32[2]{0:T(128)} %param.35) | copy-start | bytes 28
  7.2 23.4 %copy-start.15 = (bf16[2048,8]{0,1:T(8,128)(2,1)S(1)}, bf16[2048,8]{0,1:T(8,128)(2,1)}, u32[]{:S(2)}) copy-start(bf16[2048,8]{0,1:T(8,128)(2,1)} %param.33) | copy-start | bytes 98308
  7.2 23.6 %copy-start.13 = (f32[2]{0:T(128)S(1)}, f32[2]{0:T(128)}, u32[]{:S(2)}) copy-start(f32[2]{0:T(128)} %param.34) | copy-start | bytes 28
  7.2 24.0 %copy-start.2 = (f32[32,2,64,128]{3,2,1,0:T(8,128)S(1)}, f32[32,2,64,128]{3,2,1,0:T(8,128)}, u32[]{:S(2)}) copy-start(f32[32,2,64,128]{3,2,1,0:T(8,128)} %param.38) | copy-start | bytes 6291460
  7.2 92.5 %all-gather.7.cloned.1.call-start = ((), (), s32[]{:S(2)}) async-start(), calls=%async_computation.10 | async-start | bytes 1179648 | tf_op jit(solution)/shard_map/all_gather | solution.py:68
  21.7 122.8 %all-gather.5.cloned.1.call-start = ((), (), s32[]{:S(2)}) async-start(), calls=%async_computation.9 | async-start | bytes 4259840 | tf_op jit(solution)/shard_map/all_gather | solution.py:61
  31.2 2.3 %copy-start.18 = (bf16[128]{0:T(256)(128)(2,1)S(1)}, bf16[128]{0:T(256)(128)(2,1)}, u32[]{:S(2)}) copy-start(bf16[128]{0:T(256)(128)(2,1)} %param.39) | copy-start | bytes 772
  33.3 7.0 %copy-start.8 = (s32[32,4]{0,1:T(4,128)S(1)}, s32[32,4]{0,1:T(4,128)}, u32[]{:S(2)}) copy-start(s32[32,4]{0,1:T(4,128)} %param.45) | copy-start | bytes 1540
  33.3 7.3 %copy-start.9 = (bf16[2048]{0:T(1024)(128)(2,1)S(1)}, bf16[2048]{0:T(1024)(128)(2,1)}, u32[]{:S(2)}) copy-start(bf16[2048]{0:T(1024)(128)(2,1)} %param.41) | copy-start | bytes 12292
  33.4 7.3 %copy-start.10 = (bf16[2048]{0:T(1024)(128)(2,1)S(1)}, bf16[2048]{0:T(1024)(128)(2,1)}, u32[]{:S(2)}) copy-start(bf16[2048]{0:T(1024)(128)(2,1)} %param.42) | copy-start | bytes 12292
  36.0 12.4 %all-to-all-start = ((bf16[4,32,2048]{2,1,0:T(8,128)(2,1)}), bf16[4,32,2048]{2,1,0:T(8,128)(2,1)S(1)}, u32[]{:S(2)}, u32[]{:S(2)}) async-start(bf16[4,32,2048]{2,1,0:T(8,128)(2,1)} %broadcast_in_dim.25), calls=%async_computation | async-start | bytes 1048576 | tf_op jit(solution)/shard_map/all_to_all | solution.py:13
  91.4 1.6 copy-start.5
  92.7 1.2 copy-start.14
  96.0 4.4 %copy-start.11 = (bf16[2048]{0:T(1024)(128)(2,1)S(1)}, bf16[2048]{0:T(1024)(128)(2,1)}, u32[]{:S(2)}) copy-start(bf16[2048]{0:T(1024)(128)(2,1)} %param.49) | copy-start | bytes 12292
  96.0 4.5 %copy-start.16 = (bf16[2048,2]{0,1:T(2,128)(2,1)S(1)}, bf16[2048,2]{0,1:T(2,128)(2,1)}, u32[]{:S(2)}) copy-start(bf16[2048,2]{0,1:T(2,128)(2,1)} %param.43) | copy-start | bytes 24580
  96.0 4.6 %copy-start.6 = (bf16[2048,64]{0,1:T(8,128)(2,1)S(1)}, bf16[2048,64]{0,1:T(8,128)(2,1)}, u32[]{:S(2)}) copy-start(bf16[2048,64]{0,1:T(8,128)(2,1)} %param.44) | copy-start | bytes 786436
  96.0 18.6 %all-to-all-start.3 = ((bf16[4,64,4,512]{3,1,2,0:T(8,128)(2,1)}), bf16[4,64,4,512]{3,1,2,0:T(8,128)(2,1)S(1)}, u32[]{:S(2)}, u32[]{:S(2)}) async-start(bf16[4,64,4,512]{3,1,2,0:T(8,128)(2,1)} %bitcast.77), calls=%async_computation.3 | async-start | bytes 2097152 | tf_op jit(solution)/shard_map/all_to_all | solution.py:30
  99.7 69.1 %all-gather.9.cloned.1.call-start = ((), (), s32[]{:S(2)}) async-start(), calls=%async_computation.11 | async-start | bytes 3145728 | tf_op jit(solution)/shard_map/all_gather | solution.py:68
  119.8 26.9 %all-to-all-start.5 = ((bf16[32,2,1,4,512]{4,3,1,2,0:T(4,128)(2,1)}), bf16[32,2,1,4,512]{4,3,1,2,0:T(4,128)(2,1)S(1)}, u32[]{:S(2)}, u32[]{:S(2)}) async-start(bf16[32,2,1,4,512]{4,3,1,2,0:T(4,128)(2,1)} %copy.82), calls=%async_computation.5 | async-start | bytes 524288 | tf_op jit(solution)/shard_map/all_to_all | solution.py:44
  147.6 14.1 %all-to-all-start.7 = ((bf16[4,32,2048]{2,1,0:T(8,128)(2,1)}), bf16[4,32,2048]{2,1,0:T(8,128)(2,1)S(1)}, u32[]{:S(2)}, u32[]{:S(2)}) async-start(bf16[4,32,2048]{2,1,0:T(8,128)(2,1)} %broadcast_in_dim.37), calls=%async_computation.7 | async-start | bytes 1048576 | tf_op jit(solution)/shard_map/all_to_all | solution.py:13
  161.6 5.1 %copy-start.3 = (bf16[4,32,2048]{2,1,0:T(8,128)(2,1)}, bf16[4,32,2048]{2,1,0:T(8,128)(2,1)S(1)}, u32[]{:S(2)}) copy-start(bf16[4,32,2048]{2,1,0:T(8,128)(2,1)S(1)} %all-to-all-done.7) | copy-start | bytes 1572868
  162.6 13.2 %all-to-all-start.6 = ((bf16[4,32,2048]{2,1,0:T(8,128)(2,1)}), bf16[4,32,2048]{2,1,0:T(8,128)(2,1)}, u32[]{:S(2)}, u32[]{:S(2)}) async-start(bf16[4,32,2048]{2,1,0:T(8,128)(2,1)} %broadcast_in_dim.35), calls=%async_computation.6 | async-start | bytes 1048576 | tf_op jit(solution)/shard_map/all_to_all | solution.py:13
  168.8 1.8 copy-start.4
  170.6 12.2 %copy-start.12 = (bf16[512]{0:T(512)(128)(2,1)S(1)}, bf16[512]{0:T(512)(128)(2,1)}, u32[]{:S(2)}) copy-start(bf16[512]{0:T(512)(128)(2,1)} %param.53) | copy-start | bytes 3076
  179.5 8.4 %all-to-all-start.8 = ((f32[4,1,32]{2,1,0:T(1,128)}), f32[4,1,32]{2,1,0:T(1,128)S(1)}, u32[]{:S(2)}, u32[]{:S(2)}) async-start(f32[4,1,32]{2,1,0:T(1,128)} %broadcast_in_dim.39), calls=%async_computation.8 | async-start | bytes 4096 | tf_op jit(solution)/shard_map/all_to_all | solution.py:13
Sparse Core Ops, SparseCore 0:
  21.8 38.9 all-gather.6
  64.1 80.2 all-gather.4
  146.2 13.5 all-gather.8
where the time goes:
time: 197 us; the launch traced here: 196 us
  blocking collectives  59.1 us (30%)
  waiting for transfers between devices  57.6 us (29%)
  starting transfers between devices  24.2 us (12%)
  matrix products  14.5 us (7%)
  local copies, waits for them, and re-layouts  14.4 us (7%)
  between operations  14.3 us (7%)
  other arithmetic  12 us (6%)
    all_to_all x4, waiting for transfers between devices, sent_to_all(): lax.all_to_all(jnp.broadcast_to(array[None], (count, *array.shape)), axis...  23.4 us
    all_to_all x1, blocking collectives, on_device(): lax.all_to_all(outgoing, EP, split_axis=0, concat_axis=0, tiled=True)  22.3 us
    all_gather x1, waiting for transfers between devices, sent_together(): result = lax.all_gather(both, axis, axis=dim, tiled=True)  19.8 us
    all_to_all x1, blocking collectives, sent_to_all(): lax.all_to_all(jnp.broadcast_to(array[None], (count, *array.shape)), axis...  18.5 us
    all_to_all x4, starting transfers between devices, sent_to_all(): lax.all_to_all(jnp.broadcast_to(array[None], (count, *array.shape)), axis...  15.8 us
    all_gather x1, blocking collectives, all_blocks(): pieces = lax.all_gather(pieces, axes[k], axis=0, tiled=True)  14.3 us
    all_to_all x1, waiting for transfers between devices, sum_at_owner(): lax.all_to_all(cut_along(array, dim, count), axis, 0, 0, tiled=True)  13.7 us
    all_to_all x1, starting transfers between devices, exchange_in_order(): result = lax.all_to_all(result, axes[k], k, k, tiled=True)  4.58 us
  transfers between devices with their start and end apart: 9, of which 6 were waited for; matrix products, arithmetic and copies ran while one was open for 18% of the time, Pallas kernels for 0%

commit v1 on v0

--- a/solution.py
+++ b/solution.py
@@ -6,6 +6,13 @@
 
 EP = ("ep_0", "ep_1", "ep_2")
 norm_eps = 1e-06
+
+
+def all_by_exchange(shard, axis, along):
+    count = lax.axis_size(axis)
+    pieces = jnp.stack([shard for _ in range(count)])
+    pieces = lax.all_to_all(pieces, axis, split_axis=0, concat_axis=0)
+    return jnp.concatenate(pieces, axis=along)
 
 
 def sent_to_all(array, axis):
@@ -65,7 +72,7 @@
 def all_blocks(array, axes, sequence):
     pieces = array[None]
     for k in sequence:
-        pieces = lax.all_gather(pieces, axes[k], axis=0, tiled=True)
+        pieces = all_by_exchange(pieces, axes[k], 0)
     block = [lax.axis_size(axes[k]) for k in reversed(sequence)]
     pieces = pieces.reshape(*block, *array.shape)
     turned = sorted(range(len(sequence)), key=lambda place: sequence[len(sequence) - 1 - place])

time: 197 us -> 218 us (1.11)
  starting transfers between devices: 24.2 us -> 40.2 us
  blocking collectives: 59.1 us -> 44.2 us
  local copies, waits for them, and re-layouts: 14.4 us -> 20.5 us
  other arithmetic: 12 us -> 17.1 us
  matrix products: 14.5 us -> 18.8 us
  waiting for transfers between devices: 57.6 us -> 61.1 us
    all_to_all x0 -> x3, waiting for transfers between devices: none -> 28 us  [all_by_exchange(): pieces = lax.all_to_all(pieces, axis, split_axis=0, concat_axis=0)]
    all_gather x1, waiting for transfers between devices: 19.8 us -> 0.02 us  [sent_together(): result = lax.all_gather(both, axis, axis=dim, tiled=True)]
    all_gather x1 -> x0, blocking collectives: 14.3 us -> none  [all_blocks(): pieces = lax.all_gather(pieces, axes[k], axis=0, tiled=True)]
    all_to_all x0 -> x3, starting transfers between devices: none -> 12.5 us  [all_by_exchange(): pieces = lax.all_to_all(pieces, axis, split_axis=0, concat_axis=0)]
    all_to_all x1, waiting for transfers between devices: 0.02 us -> 7.68 us  [exchange_in_order(): result = lax.all_to_all(result, axes[k], k, k, tiled=True)]
    all_to_all x1, waiting for transfers between devices: 13.7 us -> 7.22 us  [sum_at_owner(): lax.all_to_all(cut_along(array, dim, count), axis, 0, 0, tiled=True)]
    all_to_all x4, waiting for transfers between devices: 23.4 us -> 18.1 us  [sent_to_all(): lax.all_to_all(jnp.broadcast_to(array[None], (count, *array.shape)), axis...]
    all_to_all x1, starting transfers between devices: 4.58 us -> 7.84 us  [exchange_in_order(): result = lax.all_to_all(result, axes[k], k, k, tiled=True)]
  transfers between devices with their start and end apart: 9 -> 10, of which waited for: 6 -> 9; matrix products, arithmetic and copies ran while one was open for 18% -> 20% of each run, Pallas kernels for 0% -> 0%
where the time goes in v1:
time: 218 us; the launch traced here: 216 us
  waiting for transfers between devices  61.1 us (28%)
  blocking collectives  44.2 us (20%)
  starting transfers between devices  40.2 us (18%)
  local copies, waits for them, and re-layouts  20.5 us (9%)
  matrix products  18.8 us (9%)
  other arithmetic  17.1 us (8%)
  between operations  14.6 us (7%)
    all_to_all x3, waiting for transfers between devices, all_by_exchange(): pieces = lax.all_to_all(pieces, axis, split_axis=0, concat_axis=0)  28 us
    all_to_all x1, blocking collectives, on_device(): lax.all_to_all(outgoing, EP, split_axis=0, concat_axis=0, tiled=True)  21.7 us
    all_to_all x1, blocking collectives, sent_to_all(): lax.all_to_all(jnp.broadcast_to(array[None], (count, *array.shape)), axis...  18.5 us
    all_to_all x4, waiting for transfers between devices, sent_to_all(): lax.all_to_all(jnp.broadcast_to(array[None], (count, *array.shape)), axis...  18.1 us
    all_to_all x4, starting transfers between devices, sent_to_all(): lax.all_to_all(jnp.broadcast_to(array[None], (count, *array.shape)), axis...  16.3 us
    all_to_all x3, starting transfers between devices, all_by_exchange(): pieces = lax.all_to_all(pieces, axis, split_axis=0, concat_axis=0)  12.5 us
    all_to_all x1, starting transfers between devices, exchange_in_order(): result = lax.all_to_all(result, axes[k], k, k, tiled=True)  7.84 us
    all_to_all x1, waiting for transfers between devices, exchange_in_order(): result = lax.all_to_all(result, axes[k], k, k, tiled=True)  7.68 us
  transfers between devices with their start and end apart: 10, of which 9 were waited for; matrix products, arithmetic and copies ran while one was open for 20% of the time, Pallas kernels for 0%

profile of v1, /device:TPU:32, one launch (start us, length us, event | category | flops | bytes accessed | tf_op | source)
XLA Modules:
  0.0 216.5 jit_solution(9226051589314237836)
XLA Ops:
  7.3 1.6 pad_maximum_fusion.1
  8.9 0.7 convert_element_type.93
  9.6 1.0 fusion.18
  10.6 1.4 fusion.4
  12.0 1.4 fusion.5
  13.4 1.4 fusion.6
  14.8 0.7 multiply_reduce_fusion.3
  16.3 2.1 multiply_reduce_fusion
  18.5 1.7 convolution_convert_fusion.3
  20.2 0.9 broadcast_in_dim.23
  21.1 4.3 %all-to-all-start = ((bf16[4,32,2048]{2,1,0:T(8,128)(2,1)}), bf16[4,32,2048]{2,1,0:T(8,128)(2,1)S(1)}, u32[]{:S(2)}, u32[]{:S(2)}) async-start(bf16[4,32,2048]{2,1,0:T(8,128)(2,1)} %broadcast_in_dim.23), calls=%async_computation | async-start | bytes 1048576 | tf_op jit(solution)/shard_map/all_to_all | solution.py:20
  26.3 8.6 %all-to-all-done = bf16[4,32,2048]{2,1,0:T(8,128)(2,1)S(1)} async-done(((bf16[4,32,2048]{2,1,0:T(8,128)(2,1)}), bf16[4,32,2048]{2,1,0:T(8,128)(2,1)S(1)}, u32[]{:S(2)}, u32[]{:S(2)}) %all-to-all-start) | async-done | bytes 524320 | tf_op jit(solution)/shard_map/all_to_all | solution.py:20
  34.8 0.7 stack.25
  35.5 4.5 %all-to-all-start.8 = ((bf16[4,1,32,512]{3,2,1,0:T(8,128)(2,1)}), bf16[4,1,32,512]{3,2,1,0:T(8,128)(2,1)S(1)}, u32[]{:S(2)}, u32[]{:S(2)}) async-start(bf16[4,1,32,512]{3,2,1,0:T(8,128)(2,1)} %stack.25), calls=%async_computation.8 | async-start | bytes 262144 | tf_op jit(solution)/shard_map/all_to_all | solution.py:14
  40.6 0.6 copy-done.7
  41.2 1.1 scatter_custom_fusion
  42.4 3.5 %all-to-all-done.8 = bf16[4,1,32,512]{3,2,1,0:T(8,128)(2,1)S(1)} async-done(((bf16[4,1,32,512]{3,2,1,0:T(8,128)(2,1)}), bf16[4,1,32,512]{3,2,1,0:T(8,128)(2,1)S(1)}, u32[]{:S(2)}, u32[]{:S(2)}) %all-to-all-start.8) | async-done | bytes 131104 | tf_op jit(solution)/shard_map/all_to_all | solution.py:14
  45.9 21.7 %all_to_all.61 = bf16[64,4,512]{2,1,0:T(4,128)(2,1)S(1)} all-to-all(bf16[64,4,512]{2,1,0:T(4,128)(2,1)S(1)} %reshape.202), channel_id=1, replica_groups=mesh['ep_0'=8,'ep_1'=4,'ep_2'=2,'tp'=4] {'ep_0','ep_1','ep_2'}, dimensions={0} | all-to-all | bytes 524288 | tf_op jit(solution)/shard_map/all_to_all | solution.py:194
  67.9 18.5 %all_to_all.62 = bf16[4,64,4,512]{3,2,1,0:T(4,128)(2,1)S(1)} all-to-all(bf16[4,64,4,512]{3,2,1,0:T(4,128)(2,1)S(1)} %broadcast_in_dim.26), channel_id=1, replica_groups=mesh['ep_0'=8,'ep_1'=4,'ep_2'=2,'tp'=4] {'tp'}, dimensions={0} | all-to-all | bytes 2097152 | tf_op jit(solution)/shard_map/all_to_all | solution.py:20
  86.4 1.1 stack.26
  87.5 4.3 %all-to-all-start.9 = ((bf16[8,4,32,512]{3,2,1,0:T(8,128)(2,1)}), bf16[8,4,32,512]{3,2,1,0:T(8,128)(2,1)S(1)}, u32[]{:S(2)}, u32[]{:S(2)}) async-start(bf16[8,4,32,512]{3,2,1,0:T(8,128)(2,1)} %stack.26), calls=%async_computation.9 | async-start | bytes 2097152 | tf_op jit(solution)/shard_map/all_to_all | solution.py:14
  91.8 1.4 copy.70
  93.9 0.5 copy-done.21
  95.4 1.1 copy.85
  96.5 22.5 %all-to-all-done.9 = bf16[8,4,32,512]{3,2,1,0:T(8,128)(2,1)S(1)} async-done(((bf16[8,4,32,512]{3,2,1,0:T(8,128)(2,1)}), bf16[8,4,32,512]{3,2,1,0:T(8,128)(2,1)S(1)}, u32[]{:S(2)}, u32[]{:S(2)}) %all-to-all-start.9) | async-done | bytes 1048608 | tf_op jit(solution)/shard_map/all_to_all | solution.py:14
  118.9 3.5 %all-to-all-start.3 = ((bf16[4,64,4,512]{3,1,2,0:T(8,128)(2,1)}), bf16[4,64,4,512]{3,1,2,0:T(8,128)(2,1)S(1)}, u32[]{:S(2)}, u32[]{:S(2)}) async-start(bf16[4,64,4,512]{3,1,2,0:T(8,128)(2,1)} %bitcast.79), calls=%async_computation.3 | async-start | bytes 2097152 | tf_op jit(solution)/shard_map/all_to_all | solution.py:37
  122.5 0.6 fusion.31
  123.0 0.6 reshape.222
  123.6 0.6 pad_clamp_fusion
  124.2 2.0 fusion.47
  126.4 1.5 pad_maximum_fusion
  127.9 7.2 %all-to-all-done.3 = bf16[4,64,4,512]{3,1,2,0:T(8,128)(2,1)S(1)} async-done(((bf16[4,64,4,512]{3,1,2,0:T(8,128)(2,1)}), bf16[4,64,4,512]{3,1,2,0:T(8,128)(2,1)S(1)}, u32[]{:S(2)}, u32[]{:S(2)}) %all-to-all-start.3) | async-done | bytes 1048608 | tf_op jit(solution)/shard_map/all_to_all | solution.py:37
  135.7 3.9 %all_to_all.63 = bf16[32,2,1,4,512]{4,3,0,2,1:T(4,128)(2,1)S(1)} all-to-all(bf16[32,2,1,4,512]{4,3,0,2,1:T(4,128)(2,1)S(1)} %copy.74), channel_id=1, replica_groups=mesh['ep_0'=8,'ep_1'=4,'ep_2'=2,'tp'=4] {'ep_2'}, dimensions={1} | all-to-all | bytes 524288 | tf_op jit(solution)/shard_map/all_to_all | solution.py:51
  139.6 3.8 %all-to-all-start.10 = ((bf16[2,32,32,512]{3,2,1,0:T(8,128)(2,1)}), bf16[2,32,32,512]{3,2,1,0:T(8,128)(2,1)S(1)}, u32[]{:S(2)}, u32[]{:S(2)}) async-start(bf16[2,32,32,512]{3,2,1,0:T(8,128)(2,1)} %pad_maximum_fusion), calls=%async_computation.10 | async-start | bytes 4194304 | tf_op jit(solution)/shard_map/all_to_all | solution.py:14
  143.4 0.8 copy.75
  144.2 2.1 all-to-all-done.10
  146.3 7.8 %all-to-all-start.5 = ((bf16[32,2,1,4,512]{4,3,1,2,0:T(4,128)(2,1)}), bf16[32,2,1,4,512]{4,3,1,2,0:T(4,128)(2,1)S(1)}, u32[]{:S(2)}, u32[]{:S(2)}) async-start(bf16[32,2,1,4,512]{4,3,1,2,0:T(4,128)(2,1)} %copy.75), calls=%async_computation.5 | async-start | bytes 524288 | tf_op jit(solution)/shard_map/all_to_all | solution.py:51
  154.1 0.8 select_reduce_fusion
  155.0 0.6 copy-done.13
  155.6 0.7 fusion.29
  156.3 3.0 %convolution_convert_fusion.1 = bf16[32,2048]{1,0:T(8,128)(2,1)} fusion(bf16[32,512]{1,0:T(8,128)(2,1)} %copy-done.7, bf16[2048,1024]{1,0:T(8,128)(2,1)} %all-gather.2.cloned.1.call-done), kind=kOutput, calls=%fused_computation.3 | convolution fusion | flops 67174400 | bytes 2260992 | tf_op jit(solution)/shard_map/sd,cd->sc/dot_general | solution.py:217
  159.3 7.7 %all-to-all-done.5 = bf16[32,2,1,4,512]{4,3,1,2,0:T(4,128)(2,1)S(1)} async-done(((bf16[32,2,1,4,512]{4,3,1,2,0:T(4,128)(2,1)}), bf16[32,2,1,4,512]{4,3,1,2,0:T(4,128)(2,1)S(1)}, u32[]{:S(2)}, u32[]{:S(2)}) %all-to-all-start.5) | async-done | bytes 262176 | tf_op jit(solution)/shard_map/all_to_all | solution.py:51
  166.9 1.9 broadcast_in_dim.34
  168.8 4.1 %all-to-all-start.7 = ((bf16[4,32,2048]{2,1,0:T(8,128)(2,1)}), bf16[4,32,2048]{2,1,0:T(8,128)(2,1)}, u32[]{:S(2)}, u32[]{:S(2)}) async-start(bf16[4,32,2048]{2,1,0:T(8,128)(2,1)} %broadcast_in_dim.34), calls=%async_computation.7 | async-start | bytes 1048576 | tf_op jit(solution)/shard_map/all_to_all | solution.py:20
  173.0 0.6 divide_multiply_fusion.1
  173.6 0.8 copy.76
  174.3 3.0 %convolution_convert_fusion.2 = bf16[32,2048]{1,0:T(8,128)(2,1)} fusion(bf16[32,512]{1,0:T(8,128)(2,1)} %copy-done.7, bf16[2048,1024]{1,0:T(8,128)(2,1)} %all-gather.2.cloned.1.call-done), kind=kOutput, calls=%fused_computation.4 | convolution fusion | flops 67174400 | bytes 2260992 | tf_op jit(solution)/shard_map/sd,cd->sc/dot_general | solution.py:214
  177.3 4.0 %all-to-all-done.7 = bf16[4,32,2048]{2,1,0:T(8,128)(2,1)} async-done(((bf16[4,32,2048]{2,1,0:T(8,128)(2,1)}), bf16[4,32,2048]{2,1,0:T(8,128)(2,1)}, u32[]{:S(2)}, u32[]{:S(2)}) %all-to-all-start.7) | async-done | bytes 524320 | tf_op jit(solution)/shard_map/all_to_all | solution.py:20
  181.3 1.8 broadcast_in_dim.33
  183.1 4.1 %all-to-all-start.6 = ((bf16[4,32,2048]{2,1,0:T(8,128)(2,1)}), bf16[4,32,2048]{2,1,0:T(8,128)(2,1)}, u32[]{:S(2)}, u32[]{:S(2)}) async-start(bf16[4,32,2048]{2,1,0:T(8,128)(2,1)} %broadcast_in_dim.33), calls=%async_computation.6 | async-start | bytes 1048576 | tf_op jit(solution)/shard_map/all_to_all | solution.py:20
  187.2 1.4 fusion.10
  188.6 1.5 copy.77
  190.1 1.2 reshape_reshape_reshape.3
  191.2 1.0 gather_fusion
  192.3 0.9 multiply_reduce_fusion.1
  193.2 1.2 convert_reduce_fusion
  194.4 1.0 all-to-all-done.6
  195.3 1.1 convert_reduce_fusion.1
  196.5 2.0 multiply_reduce_fusion.4
  198.5 0.6 broadcast_in_dim.35
  199.1 3.8 %all-to-all-start.11 = ((f32[4,1,32]{2,1,0:T(1,128)}), f32[4,1,32]{2,1,0:T(1,128)S(1)}, u32[]{:S(2)}, u32[]{:S(2)}) async-start(f32[4,1,32]{2,1,0:T(1,128)} %broadcast_in_dim.35), calls=%async_computation.11 | async-start | bytes 4096 | tf_op jit(solution)/shard_map/all_to_all | solution.py:20
  202.9 0.6 slice.31
  203.5 4.6 %all-to-all-done.11 = f32[4,1,32]{2,1,0:T(1,128)S(1)} async-done(((f32[4,1,32]{2,1,0:T(1,128)}), f32[4,1,32]{2,1,0:T(1,128)S(1)}, u32[]{:S(2)}, u32[]{:S(2)}) %all-to-all-start.11) | async-done | bytes 544 | tf_op jit(solution)/shard_map/all_to_all | solution.py:20
  208.1 1.5 add_convert_fusion
  (99 shorter events, 5.3 us)
Async XLA Ops:
  7.2 87.7 %copy-start = (bf16[1,256,2048]{2,1,0:T(8,128)(2,1)S(1)}, bf16[1,256,2048]{2,1,0:T(8,128)(2,1)}, u32[]{:S(2)}) copy-start(bf16[1,256,2048]{2,1,0:T(8,128)(2,1)} %param.48) | copy-start | bytes 3145732
  7.2 8.5 %copy-start.2 = (bf16[32,2048]{1,0:T(8,128)(2,1)S(1)}, bf16[32,2048]{1,0:T(8,128)(2,1)}, u32[]{:S(2)}) copy-start(bf16[32,2048]{1,0:T(8,128)(2,1)} %param.27) | copy-start | bytes 393220
  7.2 7.6 %copy-start.18 = (bf16[3,4,128]{2,1,0:T(4,128)(2,1)S(1)}, bf16[3,4,128]{2,1,0:T(4,128)(2,1)}, u32[]{:S(2)}) copy-start(bf16[3,4,128]{2,1,0:T(4,128)(2,1)} %param.36) | copy-start | bytes 9220
  7.2 7.6 %copy-start.10 = (bf16[32,3,3,128]{3,0,2,1:T(8,128)(2,1)S(1)}, bf16[32,3,3,128]{3,0,2,1:T(8,128)(2,1)}, u32[]{:S(2)}) copy-start(bf16[32,3,3,128]{3,0,2,1:T(8,128)(2,1)} %param.37) | copy-start | bytes 221188
  7.2 8.4 %copy-start.23 = (f32[2]{0:T(128)S(1)}, f32[2]{0:T(128)}, u32[]{:S(2)}) copy-start(f32[2]{0:T(128)} %param.35) | copy-start | bytes 28
  7.2 8.4 %copy-start.22 = (bf16[2048,8]{0,1:T(8,128)(2,1)S(1)}, bf16[2048,8]{0,1:T(8,128)(2,1)}, u32[]{:S(2)}) copy-start(bf16[2048,8]{0,1:T(8,128)(2,1)} %param.33) | copy-start | bytes 98308
  7.2 8.6 %copy-start.20 = (f32[2]{0:T(128)S(1)}, f32[2]{0:T(128)}, u32[]{:S(2)}) copy-start(f32[2]{0:T(128)} %param.34) | copy-start | bytes 28
  7.2 9.0 %copy-start.3 = (f32[32,2,64,128]{3,2,1,0:T(8,128)S(1)}, f32[32,2,64,128]{3,2,1,0:T(8,128)}, u32[]{:S(2)}) copy-start(f32[32,2,64,128]{3,2,1,0:T(8,128)} %param.38) | copy-start | bytes 6291460
  7.3 149.0 %all-gather.2.cloned.1.call-start = ((), (), s32[]{:S(2)}) async-start(), calls=%async_computation.12 | async-start | bytes 4259840 | tf_op jit(solution)/shard_map/all_gather | solution.py:68
  16.3 2.3 %copy-start.24 = (bf16[128]{0:T(256)(128)(2,1)S(1)}, bf16[128]{0:T(256)(128)(2,1)}, u32[]{:S(2)}) copy-start(bf16[128]{0:T(256)(128)(2,1)} %param.39) | copy-start | bytes 772
  18.4 7.0 %copy-start.12 = (s32[32,4]{0,1:T(4,128)S(1)}, s32[32,4]{0,1:T(4,128)}, u32[]{:S(2)}) copy-start(s32[32,4]{0,1:T(4,128)} %param.45) | copy-start | bytes 1540
  18.4 7.3 %copy-start.15 = (bf16[2048]{0:T(1024)(128)(2,1)S(1)}, bf16[2048]{0:T(1024)(128)(2,1)}, u32[]{:S(2)}) copy-start(bf16[2048]{0:T(1024)(128)(2,1)} %param.41) | copy-start | bytes 12292
  18.4 7.3 %copy-start.16 = (bf16[2048]{0:T(1024)(128)(2,1)S(1)}, bf16[2048]{0:T(1024)(128)(2,1)}, u32[]{:S(2)}) copy-start(bf16[2048]{0:T(1024)(128)(2,1)} %param.42) | copy-start | bytes 12292
  18.4 16.4 %copy-start.11 = (bf16[32,512]{1,0:T(8,128)(2,1)S(1)}, bf16[32,512]{1,0:T(8,128)(2,1)}, u32[]{:S(2)}) copy-start(bf16[32,512]{1,0:T(8,128)(2,1)} %param.52) | copy-start | bytes 98308
  21.1 13.8 %all-to-all-start = ((bf16[4,32,2048]{2,1,0:T(8,128)(2,1)}), bf16[4,32,2048]{2,1,0:T(8,128)(2,1)S(1)}, u32[]{:S(2)}, u32[]{:S(2)}) async-start(bf16[4,32,2048]{2,1,0:T(8,128)(2,1)} %broadcast_in_dim.23), calls=%async_computation | async-start | bytes 1048576 | tf_op jit(solution)/shard_map/all_to_all | solution.py:20
  35.5 10.4 %all-to-all-start.8 = ((bf16[4,1,32,512]{3,2,1,0:T(8,128)(2,1)}), bf16[4,1,32,512]{3,2,1,0:T(8,128)(2,1)S(1)}, u32[]{:S(2)}, u32[]{:S(2)}) async-start(bf16[4,1,32,512]{3,2,1,0:T(8,128)(2,1)} %stack.25), calls=%async_computation.8 | async-start | bytes 262144 | tf_op jit(solution)/shard_map/all_to_all | solution.py:14
  40.4 0.8 copy-start.6
  40.5 0.6 copy-start.7
  87.5 31.4 %all-to-all-start.9 = ((bf16[8,4,32,512]{3,2,1,0:T(8,128)(2,1)}), bf16[8,4,32,512]{3,2,1,0:T(8,128)(2,1)S(1)}, u32[]{:S(2)}, u32[]{:S(2)}) async-start(bf16[8,4,32,512]{3,2,1,0:T(8,128)(2,1)} %stack.26), calls=%async_computation.9 | async-start | bytes 2097152 | tf_op jit(solution)/shard_map/all_to_all | solution.py:14
  91.8 1.6 copy-start.4
  93.2 1.2 copy-start.21
  95.3 27.7 %copy-start.17 = (bf16[2048]{0:T(1024)(128)(2,1)S(1)}, bf16[2048]{0:T(1024)(128)(2,1)}, u32[]{:S(2)}) copy-start(bf16[2048]{0:T(1024)(128)(2,1)} %param.49) | copy-start | bytes 12292
  95.4 30.8 %copy-start.9 = (bf16[2048,64]{0,1:T(8,128)(2,1)S(1)}, bf16[2048,64]{0,1:T(8,128)(2,1)}, u32[]{:S(2)}) copy-start(bf16[2048,64]{0,1:T(8,128)(2,1)} %param.44) | copy-start | bytes 786436
  118.9 16.2 %all-to-all-start.3 = ((bf16[4,64,4,512]{3,1,2,0:T(8,128)(2,1)}), bf16[4,64,4,512]{3,1,2,0:T(8,128)(2,1)S(1)}, u32[]{:S(2)}, u32[]{:S(2)}) async-start(bf16[4,64,4,512]{3,1,2,0:T(8,128)(2,1)} %bitcast.79), calls=%async_computation.3 | async-start | bytes 2097152 | tf_op jit(solution)/shard_map/all_to_all | solution.py:37
  139.6 6.6 %all-to-all-start.10 = ((bf16[2,32,32,512]{3,2,1,0:T(8,128)(2,1)}), bf16[2,32,32,512]{3,2,1,0:T(8,128)(2,1)S(1)}, u32[]{:S(2)}, u32[]{:S(2)}) async-start(bf16[2,32,32,512]{3,2,1,0:T(8,128)(2,1)} %pad_maximum_fusion), calls=%async_computation.10 | async-start | bytes 4194304 | tf_op jit(solution)/shard_map/all_to_all | solution.py:14
  146.3 20.7 %all-to-all-start.5 = ((bf16[32,2,1,4,512]{4,3,1,2,0:T(4,128)(2,1)}), bf16[32,2,1,4,512]{4,3,1,2,0:T(4,128)(2,1)S(1)}, u32[]{:S(2)}, u32[]{:S(2)}) async-start(bf16[32,2,1,4,512]{4,3,1,2,0:T(4,128)(2,1)} %copy.75), calls=%async_computation.5 | async-start | bytes 524288 | tf_op jit(solution)/shard_map/all_to_all | solution.py:51
  154.9 0.6 copy-start.13
  155.6 17.4 %copy-start.14 = (f32[32,4]{0,1:T(4,128)S(1)}, f32[32,4]{0,1:T(4,128)}, u32[]{:S(2)}) copy-start(f32[32,4]{0,1:T(4,128)} %copy-done.13) | copy-start | bytes 1540
  166.9 16.1 %copy-start.5 = (bf16[32,2,1,4,512]{4,3,1,2,0:T(4,128)(2,1)}, bf16[32,2,1,4,512]{4,3,1,2,0:T(4,128)(2,1)S(1)}, u32[]{:S(2)}) copy-start(bf16[32,2,1,4,512]{4,3,1,2,0:T(4,128)(2,1)S(1)} %all-to-all-done.5) | copy-start | bytes 786436
  168.8 12.5 %all-to-all-start.7 = ((bf16[4,32,2048]{2,1,0:T(8,128)(2,1)}), bf16[4,32,2048]{2,1,0:T(8,128)(2,1)}, u32[]{:S(2)}, u32[]{:S(2)}) async-start(bf16[4,32,2048]{2,1,0:T(8,128)(2,1)} %broadcast_in_dim.34), calls=%async_computation.7 | async-start | bytes 1048576 | tf_op jit(solution)/shard_map/all_to_all | solution.py:20
  183.1 12.3 %all-to-all-start.6 = ((bf16[4,32,2048]{2,1,0:T(8,128)(2,1)}), bf16[4,32,2048]{2,1,0:T(8,128)(2,1)}, u32[]{:S(2)}, u32[]{:S(2)}) async-start(bf16[4,32,2048]{2,1,0:T(8,128)(2,1)} %broadcast_in_dim.33), calls=%async_computation.6 | async-start | bytes 1048576 | tf_op jit(solution)/shard_map/all_to_all | solution.py:20
  190.1 6.4 %copy-start.1 = (bf16[2,32,32,512]{3,2,0,1:T(8,128)(2,1)S(1)}, bf16[2,32,32,512]{3,2,0,1:T(8,128)(2,1)}, u32[]{:S(2)}) copy-start(bf16[2,32,32,512]{3,2,0,1:T(8,128)(2,1)} %copy.77) | copy-start | bytes 6291460
  193.2 9.7 %copy-start.19 = (bf16[512]{0:T(512)(128)(2,1)S(1)}, bf16[512]{0:T(512)(128)(2,1)}, u32[]{:S(2)}) copy-start(bf16[512]{0:T(512)(128)(2,1)} %param.53) | copy-start | bytes 3076
  193.2 9.7 %copy-start.8 = (bf16[32,3,4,128]{3,0,2,1:T(8,128)(2,1)S(1)}, bf16[32,3,4,128]{3,0,2,1:T(8,128)(2,1)}, u32[]{:S(2)}) copy-start(bf16[32,3,4,128]{3,0,2,1:T(8,128)(2,1)} %get-tuple-element.10) | copy-start | bytes 294916
  199.1 9.0 %all-to-all-start.11 = ((f32[4,1,32]{2,1,0:T(1,128)}), f32[4,1,32]{2,1,0:T(1,128)S(1)}, u32[]{:S(2)}, u32[]{:S(2)}) async-start(f32[4,1,32]{2,1,0:T(1,128)} %broadcast_in_dim.35), calls=%async_computation.11 | async-start | bytes 4096 | tf_op jit(solution)/shard_map/all_to_all | solution.py:20
Sparse Core Ops, SparseCore 0:
  11.4 80.8 all-gather.1
